TPU v7x, 512 devices: a whole 4x8x8 slice. The times are simulated.
512 devices in a mesh: ep: 32 (over z, x), tp: 16 (over y, core).
Axes of the slice: x: 4, y: 8, z: 8, core: 2. Of those that a mesh axis runs over, the one named last changes fastest.
Arguments:
- queries: bfloat16 [8192, 2048], P('ep', 'tp'), may hold values from -9 to 9
- key_rows: bfloat16 [8192, 2048], P('ep', 'tp'), may hold values from -9 to 9
- values: bfloat16 [8192, 2048], P('ep', 'tp'), may hold values from -6 to 6
- second_scale: float32 [16], P('tp'), may hold values from 0.3 to 0.8
- head_gain: float32 [128], replicated, may hold values from 0.1 to 1.9
- out_weight: bfloat16 [2048, 2048], P(None, 'tp'), may hold values from -0.125 to 0.125
- routed_in: bfloat16 [8192, 2048], P('ep'), may hold values from -6 to 6
- routed_gain: float32 [2048], replicated, may hold values from 0.1 to 1.9
- expert_ids: int32 [8192, 2], P('ep'), may hold values from 0 to 31, all different within a row; in each aligned block of 256 rows (0 to 255, 256 to 511, ...) at most 32 rows name the same one
- group_logits: float32 [8192, 8], P('ep'), may hold values from -6 to 6
- inner_logits: float32 [8192, 2], P('ep'), may hold values from -6 to 6
- gate_weight: bfloat16 [32, 2048, 4096], P('ep', None, 'tp'), may hold values from -0.125 to 0.125
- up_weight: bfloat16 [32, 2048, 4096], P('ep', None, 'tp'), may hold values from -0.125 to 0.125
- down_weight: bfloat16 [32, 4096, 2048], P('ep', 'tp'), may hold values from -0.09375 to 0.09375
Outputs:
- mixer_out: bfloat16 [8192, 2048], P('ep', 'tp')
- routed_out: bfloat16 [8192, 2048], P('ep', 'tp')
Inputs may be any that keep to these rules, and one draw needn't show every extreme that they name: `expert_ids`: the two ids of a row differ. In the rows of one device (aligned blocks of 256 rows) no expert is named by more than 32 rows, a bound that some block reaches.
All inputs are finite; a program needn't handle non-finite values.
Results may differ from a plain program's by a relative error of at most 0.018.
Values may be sent and summed in bfloat16 or wider, within the bound.
A program may use at most 128 MiB of HBM per device.

v0:
```python
import math
import jax
import jax.numpy as jnp
from jax import lax
from jax.sharding import Mesh
from jax.sharding import PartitionSpec as P

GROUP_SIZE = 4
EP = ("ep_0", "ep_1")
EPSILON = 1e-05
LOWEST = -1e30


def whole_of(array, axes, dim):
    if not axes:
        return array
    nearer = lax.all_gather(array, axes[-1], axis=dim, tiled=True)
    return whole_of(nearer, axes[:-1], dim)


def token_mixer(queries, key_rows, values, second_scale, head_gain, out_weight):
    row_count = queries.shape[0]
    local_heads = second_scale.shape[0]
    qk_size = queries.shape[1] // (2 * local_heads)
    value_size = values.shape[1] // local_heads
    first_pos = lax.axis_index(EP) * row_count
    query_pos = first_pos + jnp.arange(row_count, dtype=jnp.int32)
    last_pos = first_pos + row_count - 1
    query_four = queries.reshape(row_count, local_heads, 2, qk_size)
    score_scale = qk_size ** (-0.5)
    initial = (
        jnp.full((row_count, local_heads, 2), LOWEST, jnp.float32),
        jnp.zeros((row_count, local_heads, 2), jnp.float32),
        jnp.zeros((row_count, local_heads, 2, value_size), jnp.float32),
    )
    state_now = initial
    key_piece = whole_of(key_rows, EP, 0)
    value_piece = whole_of(values, EP, 0)
    piece_count = key_piece.shape[0]
    block_width = math.gcd(piece_count, 512)
    blocks = piece_count // block_width
    key_blocks = key_piece.reshape(blocks, block_width, local_heads, 2, qk_size)
    value_blocks = value_piece.reshape(blocks, block_width, local_heads, value_size)

    def update(state_inner, block_index):
        key_start = block_index * block_width

        def attend(inner_state):
            running_max, denominator, weighted = inner_state
            scores = (
                jnp.einsum(
                    "qhmd,khmd->qhmk",
                    query_four,
                    key_blocks[block_index],
                    preferred_element_type=jnp.float32,
                )
                * score_scale
            )
            key_pos = key_start + jnp.arange(block_width, dtype=jnp.int32)
            visible = (query_pos[:, None] >= key_pos[None, :])[:, None, None, :]
            scores = jnp.where(visible, scores, LOWEST)
            new_max = jnp.maximum(running_max, jnp.max(scores, axis=-1))
            exp_terms = jnp.where(visible, jnp.exp(scores - new_max[..., None]), 0.0)
            factor = jnp.exp(running_max - new_max)
            denominator = denominator * factor + jnp.sum(exp_terms, axis=-1)
            weighted = weighted * factor[..., None] + jnp.einsum(
                "qhmk,khe->qhme",
                exp_terms.astype(jnp.bfloat16),
                value_blocks[block_index],
                preferred_element_type=jnp.float32,
            )
            return (new_max, denominator, weighted)

        return (
            lax.cond(key_start <= last_pos, attend, lambda inner_state: inner_state, state_inner),
            None,
        )

    state_now, _ = lax.scan(update, state_now, jnp.arange(blocks, dtype=jnp.int32))
    running_max, denominator, weighted = state_now
    mapped = weighted / denominator[..., None]
    difference = mapped[:, :, 0] - second_scale[None, :, None] * mapped[:, :, 1]
    inv_norm = lax.rsqrt(jnp.mean(difference * difference, axis=-1, keepdims=True) + EPSILON)
    head_out = (
        (difference * inv_norm * head_gain)
        .astype(jnp.bfloat16)
        .reshape(row_count, local_heads * value_size)
    )
    mixed = jnp.dot(
        lax.all_gather(head_out, "tp", axis=1, tiled=True),
        out_weight,
        preferred_element_type=jnp.float32,
    )
    return mixed.astype(jnp.bfloat16)


def expert_block(
    routed_in,
    routed_gain,
    expert_ids,
    group_logits,
    inner_logits,
    gate_weight,
    up_weight,
    down_weight,
):
    token_count = routed_in.shape[0]
    chosen = expert_ids.shape[1]
    ep_size = lax.axis_size(EP)
    capacity = 2 * chosen * token_count // ep_size
    source = routed_in.astype(jnp.float32)
    normed = (
        source
        * lax.rsqrt(jnp.mean(source * source, axis=-1, keepdims=True) + EPSILON)
        * routed_gain
    ).astype(jnp.bfloat16)
    flat_ids = expert_ids.reshape(-1)
    picked = (flat_ids[:, None] == jnp.arange(ep_size, dtype=jnp.int32)[None, :]).astype(jnp.int32)
    slot_index = jnp.sum(jnp.cumsum(picked, axis=0) * picked, axis=1) - 1
    place_index = flat_ids * capacity + slot_index
    owner_row = jnp.arange(token_count * chosen, dtype=jnp.int32) // chosen
    slot_rows = jnp.zeros((ep_size * capacity,), jnp.int32).at[place_index].set(owner_row)
    outgoing = normed[slot_rows].reshape(ep_size, capacity, normed.shape[1])
    gate_local = gate_weight[0]
    up_local = up_weight[0]
    down_local = down_weight[0]
    columns = outgoing.shape[2] // lax.axis_size("tp")
    own_columns = lax.dynamic_slice_in_dim(outgoing, lax.axis_index("tp") * columns, columns, 2)
    arrived = lax.all_to_all(own_columns, EP, split_axis=0, concat_axis=0, tiled=True)
    experts_arrived = lax.all_gather(arrived, "tp", axis=2, tiled=True)
    stacked = experts_arrived.reshape(-1, experts_arrived.shape[2])
    gate_act = jnp.dot(stacked, gate_local, preferred_element_type=jnp.float32)
    up_act = jnp.dot(stacked, up_local, preferred_element_type=jnp.float32)
    hidden = (jax.nn.silu(gate_act) * up_act).astype(jnp.bfloat16)
    partial_value = jnp.dot(hidden, down_local, preferred_element_type=jnp.float32)
    partial_value = partial_value.reshape(
        experts_arrived.shape[0], experts_arrived.shape[1], partial_value.shape[1]
    )
    answered = lax.psum_scatter(
        partial_value.astype(jnp.bfloat16), "tp", scatter_dimension=2, tiled=True
    )
    returned = lax.all_to_all(answered, EP, split_axis=0, concat_axis=0, tiled=True)
    pair_out = returned.reshape(ep_size * capacity, returned.shape[2])[place_index]
    pair_out = pair_out.reshape(token_count, chosen, returned.shape[2])
    group_prob = jax.nn.softmax(group_logits, axis=-1)
    member = (
        expert_ids[..., None] // GROUP_SIZE == jnp.arange(group_logits.shape[1], dtype=jnp.int32)
    ).astype(jnp.float32)
    group_pick = jnp.sum(group_prob[:, None, :] * member, axis=-1)
    route_weight = group_pick * jax.nn.softmax(inner_logits, axis=-1)
    return jnp.sum(route_weight[..., None] * pair_out.astype(jnp.float32), axis=1).astype(
        jnp.bfloat16
    )


def local(
    queries,
    key_rows,
    values,
    second_scale,
    head_gain,
    out_weight,
    routed_in,
    routed_gain,
    expert_ids,
    group_logits,
    inner_logits,
    gate_weight,
    up_weight,
    down_weight,
):
    mixer_out = token_mixer(queries, key_rows, values, second_scale, head_gain, out_weight)
    routed_out = expert_block(
        routed_in,
        routed_gain,
        expert_ids,
        group_logits,
        inner_logits,
        gate_weight,
        up_weight,
        down_weight,
    )
    return (mixer_out, routed_out)


def solution(mesh):
    finer = Mesh(mesh.devices.reshape(8, 4, mesh.shape["tp"]), ("ep_0", "ep_1", "tp"))
    placed = (
        P(EP, "tp"),
        P(EP, "tp"),
        P(EP, "tp"),
        P("tp"),
        P(),
        P(None, "tp"),
        P(EP, None),
        P(),
        P(EP, None),
        P(EP, None),
        P(EP, None),
        P(EP, None, "tp"),
        P(EP, None, "tp"),
        P(EP, "tp", None),
    )
    return jax.shard_map(
        local, mesh=finer, in_specs=placed, out_specs=(P(EP, "tp"), P(EP, "tp")), check_vma=False
    )
```

profile of v0, /device:TPU:1, one launch (start us, length us, event | category | flops | bytes accessed | tf_op | source)
XLA Modules:
  0.0 325.3 jit_solution(6230517476498490236)
XLA Ops:
  11.0 2.4 scatter_custom_fusion
  13.5 1.5 fusion.21
  15.0 1.5 fusion.23
  16.6 6.0 %gather_fusion = bf16[1024,2048]{1,0:T(8,128)(2,1)} fusion(bf16[256,2048]{1,0:T(8,128)(2,1)S(1)} %fusion.23, s32[1024]{0:T(1024)S(1)} %fusion.38), kind=kCustom, calls=%fused_computation | custom fusion | bytes 8392704 | tf_op jit(solution)/shard_map/gather | solution.py:123
  23.5 24.9 %all_to_all.10 = bf16[32,32,128]{2,1,0:T(8,128)(2,1)} all-to-all(bf16[32,32,128]{2,1,0:T(8,128)(2,1)S(1)} %constant_dynamic-slice_fusion), channel_id=1, replica_groups=mesh['ep_0'=8,'ep_1'=4,'tp'=16] {'ep_0','ep_1'}, dimensions={0} | all-to-all | bytes 524288 | tf_op jit(solution)/shard_map/all_to_all | solution.py:129
  48.6 10.7 %all_gather.18 = bf16[1024,128]{1,0:T(8,128)(2,1)} all-gather(bf16[256,128]{1,0:T(8,128)(2,1)S(1)} %copy-done.3), channel_id=1, replica_groups=mesh['ep_0'=8,'ep_1'=4,'tp'=16] {'ep_1'}, dimensions={0}, use_global_device_ids=true | all-gather | bytes 327680 | tf_op jit(solution)/shard_map/all_gather | solution.py:17
  59.4 11.1 %all_gather.20 = bf16[1024,128]{1,0:T(8,128)(2,1)} all-gather(bf16[256,128]{1,0:T(8,128)(2,1)S(1)} %copy-done.4), channel_id=1, replica_groups=mesh['ep_0'=8,'ep_1'=4,'tp'=16] {'ep_1'}, dimensions={0}, use_global_device_ids=true | all-gather | bytes 327680 | tf_op jit(solution)/shard_map/all_gather | solution.py:17
  70.6 28.3 %all-gather.11.cloned.1.call-done = bf16[32,32,2048]{2,1,0:T(8,128)(2,1)} async-done(((bf16[32,32,128]{2,1,0:T(8,128)(2,1)}), bf16[32,32,2048]{2,1,0:T(8,128)(2,1)}) %all-gather.11.cloned.1.call-update) | async-done | bytes 4194320 | tf_op jit(solution)/shard_map/all_gather | solution.py:130
  98.8 3.6 %fusion.27 = f32[1024,256]{1,0:T(8,128)S(1)} fusion(bf16[1024,2048]{1,0:T(8,128)(2,1)} %bitcast.107, bf16[1,2048,256]{2,1,0:T(8,128)(2,1)S(1)} %copy-done.9), kind=kOutput, calls=%fused_computation.42 | convolution fusion | flops 1073741824 | bytes 6291456 | tf_op jit(solution)/shard_map/dot_general | solution.py:132
  103.7 3.2 convolution_convert_fusion
  106.9 23.0 %copy.58 = bf16[32,32,2048]{1,0,2:T(8,128)(2,1)} copy(bf16[32,32,2048]{2,1,0:T(8,128)(2,1)} %convolution_convert_fusion) | data formatting | bytes 8388608
  130.0 23.3 %reshape.280 = bf16[2048,1024]{1,0:T(8,128)(2,1)} reshape(bf16[2048,32,32]{2,1,0:T(8,128)(2,1)} %bitcast.93) | data formatting | bytes 8388608
  154.9 8.2 %reshape.279 = bf16[16,512,1,2,64]{4,3,1,0,2:T(2,128)(2,1)} reshape(bf16[8192,128]{1,0:T(8,128)(2,1)} %all-gather.5.cloned.1.call-done) | data formatting | bytes 4194304 | tf_op jit(solution)/shard_map/reshape | solution.py:42
  163.1 9.1 %copy.48 = bf16[16,512,1,2,64]{1,4,3,2,0:T(8,128)(2,1)S(1)} copy(bf16[16,512,1,2,64]{4,3,1,0,2:T(2,128)(2,1)} %reshape.279) | data formatting | bytes 4194304
  172.2 10.3 %all-gather.7.cloned.1.call-done = bf16[8192,128]{1,0:T(8,128)(2,1)} async-done(((bf16[1024,128]{1,0:T(8,128)(2,1)}), bf16[8192,128]{1,0:T(8,128)(2,1)}) %all-gather.7.cloned.1.call-update) | async-done | bytes 2097168 | tf_op jit(solution)/shard_map/all_gather | solution.py:17
  182.6 3.9 %copy.49 = bf16[16,512,1,128]{1,3,2,0:T(8,128)(2,1)} copy(bf16[16,512,1,128]{3,1,0,2:T(8,128)(2,1)} %bitcast.98) | data formatting | bytes 4194304
  186.6 24.3 %while.15 = (s32[]{:T(128)}, f32[256,1,2]{0,2,1:T(2,128)S(1)}, f32[256,1,2]{0,2,1:T(2,128)S(1)}, f32[256,1,2,128]{0,3,2,1:T(8,128)S(1)}, s32[16]{0:T(128)S(1)}, ...) while((s32[]{:T(128)}, f32[256,1,2]{0,2,1:T(2,128)S(1)}, ...), condition=%wide.region_5.6_spmd.clone, body=%wide.region_0.5_spmd.clone.sunk | while | flops 103287040 | bytes 4563285 | solution.py:79
  187.8 4.0 %conditional.3 = ((f32[256,1,2]{0,2,1:T(2,128)S(1)}, f32[256,1,2]{0,2,1:T(2,128)S(1)}, f32[256,1,2,128]{0,3,2,1:T(8,128)S(1)})) conditional(s32[]{:T(128)} %convert_element_type.73, (f32[256,1,2]{0,2,1:T(2,128)S(1)}, f32[256,1,2]{0,2,1:T(2,128)S(1)}, f32[256,1,2,128]{0,3,2,1:T(8,128)S(1)}) %tuple.42, (s32[]{:T(128)}, s32[]{:T(128)}, s32[]{:T(128)}, ...), branch_computations={%region_1.1_spmd, %region_2.4_spmd} | conditional | flops 103287040 | bytes 4562002 | solution.py:75
  211.9 39.5 %reduce-scatter.4.cloned.1.call-done = bf16[128,1024]{1,0:T(8,128)(2,1)} async-done(((bf16[2048,1024]{1,0:T(8,128)(2,1)}), bf16[128,1024]{1,0:T(8,128)(2,1)}) %reduce-scatter.4.cloned.1.call-update) | async-done | bytes 262160
  251.4 1.8 reshape.281
  253.3 1.8 copy.59
  255.1 25.9 %all-to-all-start.1 = ((bf16[32,32,128]{2,1,0:T(8,128)(2,1)}), bf16[32,32,128]{2,1,0:T(8,128)(2,1)S(1)}, u32[]{:S(2)}, u32[]{:S(2)}) async-start(bf16[32,32,128]{2,1,0:T(8,128)(2,1)} %copy.59), calls=%async_computation.1 | async-start | bytes 524288 | tf_op jit(solution)/shard_map/all_to_all | solution.py:142
  281.1 32.9 %all-gather.9.cloned.1.call-done = bf16[256,2048]{0,1:T(8,128)(2,1)} async-done(((bf16[256,128]{0,1:T(8,128)(2,1)}), bf16[256,2048]{0,1:T(8,128)(2,1)}) %all-gather.9.cloned.1.call-update) | async-done | bytes 1048592 | tf_op jit(solution)/shard_map/all_gather | solution.py:90
  314.0 2.3 convolution_convert_fusion.1
  (129 shorter events, 22.5 us)
Async XLA Ops:
  7.2 96.6 %copy-start = (bf16[1,256,2048]{2,1,0:T(8,128)(2,1)S(1)}, bf16[1,256,2048]{2,1,0:T(8,128)(2,1)}, u32[]{:S(2)}) copy-start(bf16[1,256,2048]{2,1,0:T(8,128)(2,1)} %param.31) | copy-start | bytes 3145732
  7.2 91.6 %all-gather.11.cloned.1.call-start = ((), (), s32[]{:S(2)}) async-start(), calls=%async_computation.6 | async-start | bytes 4456448 | tf_op jit(solution)/shard_map/all_gather | solution.py:130
  16.5 32.0 %copy-start.3 = (bf16[256,128]{1,0:T(8,128)(2,1)S(1)}, bf16[256,128]{1,0:T(8,128)(2,1)}, u32[]{:S(2)}) copy-start(bf16[256,128]{1,0:T(8,128)(2,1)} %param.19) | copy-start | bytes 196612
  16.5 42.8 %copy-start.4 = (bf16[256,128]{1,0:T(8,128)(2,1)S(1)}, bf16[256,128]{1,0:T(8,128)(2,1)}, u32[]{:S(2)}) copy-start(bf16[256,128]{1,0:T(8,128)(2,1)} %param.20) | copy-start | bytes 196612
  16.5 82.3 %copy-start.9 = (bf16[1,2048,256]{2,1,0:T(8,128)(2,1)S(1)}, bf16[1,2048,256]{2,1,0:T(8,128)(2,1)}, u32[]{:S(2)}) copy-start(bf16[1,2048,256]{2,1,0:T(8,128)(2,1)} %param.29) | copy-start | bytes 3145732
  48.5 106.4 %all-gather.5.cloned.1.call-start = ((), (), s32[]{:S(2)}) async-start(), calls=%async_computation.3 | async-start | bytes 2359296 | tf_op jit(solution)/shard_map/all_gather | solution.py:17
  59.3 43.2 %copy-start.10 = (bf16[1,2048,256]{2,1,0:T(8,128)(2,1)S(1)}, bf16[1,2048,256]{2,1,0:T(8,128)(2,1)}, u32[]{:S(2)}) copy-start(bf16[1,2048,256]{2,1,0:T(8,128)(2,1)} %param.30) | copy-start | bytes 3145732
  59.3 123.3 %all-gather.7.cloned.1.call-start = ((), (), s32[]{:S(2)}) async-start(), calls=%async_computation.4 | async-start | bytes 2359296 | tf_op jit(solution)/shard_map/all_gather | solution.py:17
  70.5 180.9 %reduce-scatter.4.cloned.1.call-start = ((), (), s32[]{:S(2)}) async-start(), calls=%async_computation.7 | async-start | bytes 4456448
  98.8 3.6 %copy-start.8 = (bf16[32,32,2048]{2,1,0:T(8,128)(2,1)S(1)}, bf16[32,32,2048]{2,1,0:T(8,128)(2,1)}, u32[]{:S(2)}) copy-start(bf16[32,32,2048]{2,1,0:T(8,128)(2,1)} %all-gather.11.cloned.1.call-done) | copy-start | bytes 12582916
  153.3 0.8 copy-start.5
  153.3 160.7 %all-gather.9.cloned.1.call-start = ((), (), s32[]{:S(2)}) async-start(), calls=%async_computation.5 | async-start | bytes 1114112 | tf_op jit(solution)/shard_map/all_gather | solution.py:90
  186.5 24.4 %copy-start.7 = (f32[128]{0:T(128)S(1)}, f32[128]{0:T(128)}, u32[]{:S(2)}) copy-start(f32[128]{0:T(128)} %param.22) | copy-start | bytes 1540
  186.6 25.2 %copy-start.2 = (f32[256,8]{0,1:T(8,128)S(1)}, f32[256,8]{0,1:T(8,128)}, u32[]{:S(2)}) copy-start(f32[256,8]{0,1:T(8,128)} %param.27) | copy-start | bytes 24580
  186.6 25.2 %copy-start.6 = (f32[256,2]{0,1:T(2,128)S(1)}, f32[256,2]{0,1:T(2,128)}, u32[]{:S(2)}) copy-start(f32[256,2]{0,1:T(2,128)} %param.28) | copy-start | bytes 6148
  210.9 103.1 %copy-start.1 = (bf16[2048,128]{1,0:T(8,128)(2,1)S(1)}, bf16[2048,128]{1,0:T(8,128)(2,1)}, u32[]{:S(2)}) copy-start(bf16[2048,128]{1,0:T(8,128)(2,1)} %param.23) | copy-start | bytes 1572868
  255.1 61.3 %all-to-all-start.1 = ((bf16[32,32,128]{2,1,0:T(8,128)(2,1)}), bf16[32,32,128]{2,1,0:T(8,128)(2,1)S(1)}, u32[]{:S(2)}, u32[]{:S(2)}) async-start(bf16[32,32,128]{2,1,0:T(8,128)(2,1)} %copy.59), calls=%async_computation.1 | async-start | bytes 524288 | tf_op jit(solution)/shard_map/all_to_all | solution.py:142
Sparse Core Ops, SparseCore 0:
  48.6 50.1 all-gather.10
  100.9 37.4 all-gather.4
  140.5 42.0 all-gather.6
  185.3 66.1 reduce-scatter.3
  254.0 59.9 all-gather.8
where the time goes:
time: 328 us; the launch traced here: 325 us
  waiting for transfers between devices  111 us (34%)
  local copies, waits for them, and re-layouts  94.1 us (29%)
  blocking collectives  46.8 us (14%)
  starting transfers between devices  26.3 us (8%)
  between operations  14.8 us (5%)
  loops' own time  12.6 us (4%)
  matrix products  12.1 us (4%)
  other arithmetic  7.48 us (2%)
    unnamed x30, local copies, waits for them, and re-layouts  64.6 us
    unnamed x6, waiting for transfers between devices  39.6 us
    all_gather x1, waiting for transfers between devices, token_mixer(): lax.all_gather(head_out, 'tp', axis=1, tiled=True)  32.9 us
    all_gather x1, waiting for transfers between devices, expert_block(): experts_arrived = lax.all_gather(arrived, 'tp', axis=2, tiled=True)  28.3 us
    all_to_all x1, starting transfers between devices, expert_block(): lax.all_to_all(answered, EP, split_axis=0, concat_axis=0, tiled=True)  25.9 us
    all_to_all x1, blocking collectives, expert_block(): lax.all_to_all(own_columns, EP, split_axis=0, concat_axis=0, tiled=True)  24.9 us
    all_gather x2, blocking collectives, whole_of(): nearer = lax.all_gather(array, axes[-1], axis=dim, tiled=True)  21.8 us
    another operation x1, loops' own time, token_mixer(): lax.scan(update, state_now, jnp.arange(blocks, dtype=jnp.int32))  10.6 us
  transfers between devices with their start and end apart: 6, of which 4 were waited for; matrix products, arithmetic and copies ran while one was open for 29% of the time, Pallas kernels for 0%

commit v1 on v0

--- a/solution.py
+++ b/solution.py
@@ -86,11 +86,12 @@
         .astype(jnp.bfloat16)
         .reshape(row_count, local_heads * value_size)
     )
-    mixed = jnp.dot(
-        lax.all_gather(head_out, "tp", axis=1, tiled=True),
-        out_weight,
-        preferred_element_type=jnp.float32,
-    )
+
+    def feed_view_up(in_array):
+        all_rows = jnp.concatenate([in_array for _ in range(jax.lax.psum(1, "tp"))], axis=1)
+        return jax.lax.all_to_all(all_rows, "tp", 1, 1, tiled=True)
+
+    mixed = jnp.dot(feed_view_up(head_out), out_weight, preferred_element_type=jnp.float32)
     return mixed.astype(jnp.bfloat16)
 
 

time: 328 us -> 341 us (1.040)
  starting transfers between devices: 26.3 us -> 56.6 us
  waiting for transfers between devices: 111 us -> 91.9 us
    all_gather x1 -> x0, waiting for transfers between devices: 32.9 us -> none  [token_mixer(): lax.all_gather(head_out, 'tp', axis=1, tiled=True)]
    all_to_all x1, starting transfers between devices: 25.9 us -> 45.1 us  [expert_block(): lax.all_to_all(answered, EP, split_axis=0, concat_axis=0, tiled=True)]
    all_to_all x0 -> x1, starting transfers between devices: none -> 11.2 us  [feed_view_up(): return jax.lax.all_to_all(all_rows, 'tp', 1, 1, tiled=True)]
    all_to_all x1, waiting for transfers between devices: 0.01 us -> 8.67 us  [expert_block(): lax.all_to_all(answered, EP, split_axis=0, concat_axis=0, tiled=True)]
    unnamed x6 -> x5, waiting for transfers between devices: 39.6 us -> 44.7 us
    unnamed x30 -> x28, local copies, waits for them, and re-layouts: 64.6 us -> 64.8 us
where the time goes in v1:
time: 341 us; the launch traced here: 339 us
  local copies, waits for them, and re-layouts  97 us (28%)
  waiting for transfers between devices  91.9 us (27%)
  starting transfers between devices  56.6 us (17%)
  blocking collectives  46.8 us (14%)
  between operations  14.8 us (4%)
  loops' own time  12.6 us (4%)
  matrix products  12.2 us (4%)
  other arithmetic  6.86 us (2%)
    unnamed x28, local copies, waits for them, and re-layouts  64.8 us
    all_to_all x1, starting transfers between devices, expert_block(): lax.all_to_all(answered, EP, split_axis=0, concat_axis=0, tiled=True)  45.1 us
    unnamed x5, waiting for transfers between devices  44.7 us
    all_gather x1, waiting for transfers between devices, expert_block(): experts_arrived = lax.all_gather(arrived, 'tp', axis=2, tiled=True)  28.1 us
    all_to_all x1, blocking collectives, expert_block(): lax.all_to_all(own_columns, EP, split_axis=0, concat_axis=0, tiled=True)  24.9 us
    all_gather x2, blocking collectives, whole_of(): nearer = lax.all_gather(array, axes[-1], axis=dim, tiled=True)  21.8 us
    all_to_all x1, starting transfers between devices, feed_view_up(): return jax.lax.all_to_all(all_rows, 'tp', 1, 1, tiled=True)  11.2 us
    another operation x1, loops' own time, token_mixer(): lax.scan(update, state_now, jnp.arange(blocks, dtype=jnp.int32))  10.6 us
  transfers between devices with their start and end apart: 6, of which 4 were waited for; matrix products, arithmetic and copies ran while one was open for 29% of the time, Pallas kernels for 0%

profile of v1, /device:TPU:1, one launch (start us, length us, event | category | flops | bytes accessed | tf_op | source)
XLA Modules:
  0.0 338.8 jit_solution(11611852328548836392)
XLA Ops:
  11.0 2.4 scatter_custom_fusion
  15.0 1.5 fusion.23
  16.6 6.0 %gather_fusion = bf16[1024,2048]{1,0:T(8,128)(2,1)} fusion(bf16[256,2048]{1,0:T(8,128)(2,1)S(1)} %fusion.23, s32[1024]{0:T(1024)S(1)} %fusion.38), kind=kCustom, calls=%fused_computation | custom fusion | bytes 8392704 | tf_op jit(solution)/shard_map/gather | solution.py:124
  23.5 24.9 %all_to_all.19 = bf16[32,32,128]{2,1,0:T(8,128)(2,1)} all-to-all(bf16[32,32,128]{2,1,0:T(8,128)(2,1)S(1)} %constant_dynamic-slice_fusion), channel_id=1, replica_groups=mesh['ep_0'=8,'ep_1'=4,'tp'=16] {'ep_0','ep_1'}, dimensions={0} | all-to-all | bytes 524288 | tf_op jit(solution)/shard_map/all_to_all | solution.py:130
  48.6 10.7 %all_gather.15 = bf16[1024,128]{1,0:T(8,128)(2,1)} all-gather(bf16[256,128]{1,0:T(8,128)(2,1)S(1)} %copy-done.2), channel_id=1, replica_groups=mesh['ep_0'=8,'ep_1'=4,'tp'=16] {'ep_1'}, dimensions={0}, use_global_device_ids=true | all-gather | bytes 327680 | tf_op jit(solution)/shard_map/all_gather | solution.py:17
  59.4 11.1 %all_gather.17 = bf16[1024,128]{1,0:T(8,128)(2,1)} all-gather(bf16[256,128]{1,0:T(8,128)(2,1)S(1)} %copy-done.3), channel_id=1, replica_groups=mesh['ep_0'=8,'ep_1'=4,'tp'=16] {'ep_1'}, dimensions={0}, use_global_device_ids=true | all-gather | bytes 327680 | tf_op jit(solution)/shard_map/all_gather | solution.py:17
  70.7 28.1 %all-gather.8.cloned.1.call-done = bf16[32,32,2048]{2,1,0:T(8,128)(2,1)} async-done(((bf16[32,32,128]{2,1,0:T(8,128)(2,1)}), bf16[32,32,2048]{2,1,0:T(8,128)(2,1)}) %all-gather.8.cloned.1.call-update) | async-done | bytes 4194320 | tf_op jit(solution)/shard_map/all_gather | solution.py:131
  98.8 3.6 %fusion.27 = f32[1024,256]{1,0:T(8,128)S(1)} fusion(bf16[1024,2048]{1,0:T(8,128)(2,1)} %bitcast.109, bf16[1,2048,256]{2,1,0:T(8,128)(2,1)S(1)} %copy-done.8), kind=kOutput, calls=%fused_computation.42 | convolution fusion | flops 1073741824 | bytes 6291456 | tf_op jit(solution)/shard_map/dot_general | solution.py:133
  103.7 3.2 convolution_convert_fusion
  106.9 23.0 %copy.77 = bf16[32,32,2048]{1,0,2:T(8,128)(2,1)} copy(bf16[32,32,2048]{2,1,0:T(8,128)(2,1)} %convolution_convert_fusion) | data formatting | bytes 8388608
  130.0 23.3 %reshape.457 = bf16[2048,1024]{1,0:T(8,128)(2,1)} reshape(bf16[2048,32,32]{2,1,0:T(8,128)(2,1)} %bitcast.94) | data formatting | bytes 8388608
  154.9 8.2 %reshape.456 = bf16[16,512,1,2,64]{4,3,1,0,2:T(2,128)(2,1)} reshape(bf16[8192,128]{1,0:T(8,128)(2,1)} %all-gather.4.cloned.1.call-done) | data formatting | bytes 4194304 | tf_op jit(solution)/shard_map/reshape | solution.py:42
  163.1 9.1 %copy.65 = bf16[16,512,1,2,64]{1,4,3,2,0:T(8,128)(2,1)S(1)} copy(bf16[16,512,1,2,64]{4,3,1,0,2:T(2,128)(2,1)} %reshape.456) | data formatting | bytes 4194304
  172.2 10.4 %all-gather.6.cloned.1.call-done = bf16[8192,128]{1,0:T(8,128)(2,1)} async-done(((bf16[1024,128]{1,0:T(8,128)(2,1)}), bf16[8192,128]{1,0:T(8,128)(2,1)}) %all-gather.6.cloned.1.call-update) | async-done | bytes 2097168 | tf_op jit(solution)/shard_map/all_gather | solution.py:17
  182.7 3.9 %copy.66 = bf16[16,512,1,128]{1,3,2,0:T(8,128)(2,1)} copy(bf16[16,512,1,128]{3,1,0,2:T(8,128)(2,1)} %bitcast.100) | data formatting | bytes 4194304
  186.7 24.3 %while.15 = (s32[]{:T(128)}, f32[256,1,2]{0,2,1:T(2,128)S(1)}, f32[256,1,2]{0,2,1:T(2,128)S(1)}, f32[256,1,2,128]{0,3,2,1:T(8,128)S(1)}, s32[16]{0:T(128)S(1)}, ...) while((s32[]{:T(128)}, f32[256,1,2]{0,2,1:T(2,128)S(1)}, ...), condition=%wide.region_5.6_spmd.clone, body=%wide.region_0.5_spmd.clone.sunk | while | flops 103287040 | bytes 4563285 | solution.py:79
  187.9 4.0 %conditional.3 = ((f32[256,1,2]{0,2,1:T(2,128)S(1)}, f32[256,1,2]{0,2,1:T(2,128)S(1)}, f32[256,1,2,128]{0,3,2,1:T(8,128)S(1)})) conditional(s32[]{:T(128)} %convert_element_type.92, (f32[256,1,2]{0,2,1:T(2,128)S(1)}, f32[256,1,2]{0,2,1:T(2,128)S(1)}, f32[256,1,2,128]{0,3,2,1:T(8,128)S(1)}) %tuple.43, (s32[]{:T(128)}, s32[]{:T(128)}, s32[]{:T(128)}, ...), branch_computations={%region_1.1_spmd, %region_2.4_spmd} | conditional | flops 103287040 | bytes 4562002 | solution.py:75
  212.5 11.2 %all-to-all-start = ((bf16[256,16,128]{2,0,1:T(8,128)(2,1)}), bf16[256,16,128]{2,0,1:T(8,128)(2,1)S(1)}, u32[]{:S(2)}, u32[]{:S(2)}) async-start(bf16[256,16,128]{2,0,1:T(8,128)(2,1)} %concatenate.4), calls=%async_computation | async-start | bytes 2097152 | tf_op jit(solution)/shard_map/all_to_all | solution.py:92
  223.8 44.7 %reduce-scatter.4.cloned.1.call-done = bf16[128,1024]{1,0:T(8,128)(2,1)} async-done(((bf16[2048,1024]{1,0:T(8,128)(2,1)}), bf16[128,1024]{1,0:T(8,128)(2,1)}) %reduce-scatter.4.cloned.1.call-update) | async-done | bytes 262160
  268.5 1.8 reshape.458
  270.3 1.8 copy.78
  272.1 45.1 %all-to-all-start.2 = ((bf16[32,32,128]{2,1,0:T(8,128)(2,1)}), bf16[32,32,128]{2,1,0:T(8,128)(2,1)S(1)}, u32[]{:S(2)}, u32[]{:S(2)}) async-start(bf16[32,32,128]{2,1,0:T(8,128)(2,1)} %copy.78), calls=%async_computation.2 | async-start | bytes 524288 | tf_op jit(solution)/shard_map/all_to_all | solution.py:143
  318.7 2.5 convolution_convert_fusion.1
  321.2 8.7 %all-to-all-done.2 = bf16[32,32,128]{2,1,0:T(8,128)(2,1)S(1)} async-done(((bf16[32,32,128]{2,1,0:T(8,128)(2,1)}), bf16[32,32,128]{2,1,0:T(8,128)(2,1)S(1)}, u32[]{:S(2)}, u32[]{:S(2)}) %all-to-all-start.2) | async-done | bytes 262176 | tf_op jit(solution)/shard_map/all_to_all | solution.py:143
  (129 shorter events, 26.2 us)
Async XLA Ops:
  7.2 96.6 %copy-start = (bf16[1,256,2048]{2,1,0:T(8,128)(2,1)S(1)}, bf16[1,256,2048]{2,1,0:T(8,128)(2,1)}, u32[]{:S(2)}) copy-start(bf16[1,256,2048]{2,1,0:T(8,128)(2,1)} %param.31) | copy-start | bytes 3145732
  7.2 91.6 %all-gather.8.cloned.1.call-start = ((), (), s32[]{:S(2)}) async-start(), calls=%async_computation.6 | async-start | bytes 4456448 | tf_op jit(solution)/shard_map/all_gather | solution.py:131
  16.5 32.0 %copy-start.2 = (bf16[256,128]{1,0:T(8,128)(2,1)S(1)}, bf16[256,128]{1,0:T(8,128)(2,1)}, u32[]{:S(2)}) copy-start(bf16[256,128]{1,0:T(8,128)(2,1)} %param.19) | copy-start | bytes 196612
  16.5 42.8 %copy-start.3 = (bf16[256,128]{1,0:T(8,128)(2,1)S(1)}, bf16[256,128]{1,0:T(8,128)(2,1)}, u32[]{:S(2)}) copy-start(bf16[256,128]{1,0:T(8,128)(2,1)} %param.20) | copy-start | bytes 196612
  16.5 82.3 %copy-start.8 = (bf16[1,2048,256]{2,1,0:T(8,128)(2,1)S(1)}, bf16[1,2048,256]{2,1,0:T(8,128)(2,1)}, u32[]{:S(2)}) copy-start(bf16[1,2048,256]{2,1,0:T(8,128)(2,1)} %param.29) | copy-start | bytes 3145732
  48.5 106.4 %all-gather.4.cloned.1.call-start = ((), (), s32[]{:S(2)}) async-start(), calls=%async_computation.4 | async-start | bytes 2359296 | tf_op jit(solution)/shard_map/all_gather | solution.py:17
  59.3 43.2 %copy-start.9 = (bf16[1,2048,256]{2,1,0:T(8,128)(2,1)S(1)}, bf16[1,2048,256]{2,1,0:T(8,128)(2,1)}, u32[]{:S(2)}) copy-start(bf16[1,2048,256]{2,1,0:T(8,128)(2,1)} %param.30) | copy-start | bytes 3145732
  59.3 123.4 %all-gather.6.cloned.1.call-start = ((), (), s32[]{:S(2)}) async-start(), calls=%async_computation.5 | async-start | bytes 2359296 | tf_op jit(solution)/shard_map/all_gather | solution.py:17
  70.5 198.0 %reduce-scatter.4.cloned.1.call-start = ((), (), s32[]{:S(2)}) async-start(), calls=%async_computation.7 | async-start | bytes 4456448
  98.8 3.6 %copy-start.7 = (bf16[32,32,2048]{2,1,0:T(8,128)(2,1)S(1)}, bf16[32,32,2048]{2,1,0:T(8,128)(2,1)}, u32[]{:S(2)}) copy-start(bf16[32,32,2048]{2,1,0:T(8,128)(2,1)} %all-gather.8.cloned.1.call-done) | copy-start | bytes 12582916
  153.3 0.8 copy-start.4
  186.7 24.4 %copy-start.6 = (f32[128]{0:T(128)S(1)}, f32[128]{0:T(128)}, u32[]{:S(2)}) copy-start(f32[128]{0:T(128)} %param.22) | copy-start | bytes 1540
  210.9 12.7 %copy-start.1 = (f32[256,8]{0,1:T(8,128)S(1)}, f32[256,8]{0,1:T(8,128)}, u32[]{:S(2)}) copy-start(f32[256,8]{0,1:T(8,128)} %param.27) | copy-start | bytes 24580
  210.9 12.7 %copy-start.5 = (f32[256,2]{0,1:T(2,128)S(1)}, f32[256,2]{0,1:T(2,128)}, u32[]{:S(2)}) copy-start(f32[256,2]{0,1:T(2,128)} %param.28) | copy-start | bytes 6148
  212.5 59.6 %all-to-all-start = ((bf16[256,16,128]{2,0,1:T(8,128)(2,1)}), bf16[256,16,128]{2,0,1:T(8,128)(2,1)S(1)}, u32[]{:S(2)}, u32[]{:S(2)}) async-start(bf16[256,16,128]{2,0,1:T(8,128)(2,1)} %concatenate.4), calls=%async_computation | async-start | bytes 2097152 | tf_op jit(solution)/shard_map/all_to_all | solution.py:92
  272.1 57.8 %all-to-all-start.2 = ((bf16[32,32,128]{2,1,0:T(8,128)(2,1)}), bf16[32,32,128]{2,1,0:T(8,128)(2,1)S(1)}, u32[]{:S(2)}, u32[]{:S(2)}) async-start(bf16[32,32,128]{2,1,0:T(8,128)(2,1)} %copy.78), calls=%async_computation.2 | async-start | bytes 524288 | tf_op jit(solution)/shard_map/all_to_all | solution.py:143
Sparse Core Ops, SparseCore 0:
  48.6 50.1 all-gather.7
  100.9 37.2 all-gather.3
  140.3 42.3 all-gather.5
  185.4 83.0 reduce-scatter.3
